TPU v7x, 32 devices: a whole 2x2x4 slice. The times are simulated.
32 devices in a mesh: sp: 8 (over z, y), tp: 4 (over x, core).
Axes of the slice: x: 2, y: 2, z: 4, core: 2. Of those that a mesh axis runs over, the one named last changes fastest.
Arguments:
- queries: bfloat16 [8192, 1024], P('sp', 'tp'), may hold values from -300 to 300
- keys: bfloat16 [8192, 512], P('sp', 'tp'), may hold values from -6 to 6
- values: bfloat16 [8192, 512], P('sp', 'tp'), may hold values from -6 to 6
- sink_logits: float32 [16], P('tp'), may hold values from 1 to 6
- residual: bfloat16 [8192, 2048], P('sp'), may hold values from -3 to 3
- out_weight: bfloat16 [1024, 2048], P('tp'), may hold values from -0.5390625 to 0.5390625
- norm_gain: float32 [2048], replicated, may hold values from 0.1 to 1.9
- gate_weight: bfloat16 [2048, 5632], P('sp', 'tp'), may hold values from -0.125 to 0.125
- up_weight: bfloat16 [2048, 5632], P('sp', 'tp'), may hold values from -0.125 to 0.125
- down_weight: bfloat16 [2048, 5632], P('sp', 'tp'), may hold values from -0.1796875 to 0.1796875
Outputs:
- layer_out: bfloat16 [8192, 2048], P(('sp', 'tp'))
All inputs are finite; a program needn't handle non-finite values.
Results may differ from a plain program's by a relative error of at most 0.02.
Values may be sent and summed in bfloat16 or wider, within the bound.
No kernel may reach another device: no remote copies, remote signals or barrier semaphores. Data moves between devices by JAX's collectives and lax.ppermute only.
A program may use at most 64 MiB of HBM per device.

v0:
```python
import jax
import jax.numpy as jnp
from jax import lax
from jax.sharding import PartitionSpec as P

QH = 16
HD = 64
WINDOW = 128


def shifted(block, axis, distance):
    devices = range(lax.axis_size(axis))
    route = [(i - distance, i) for i in devices if i - distance in devices]
    return lax.ppermute(block, axis, route)


def attend(queries, keys, values, sink_logits):
    local_rows = queries.shape[0]
    kv_local = keys.shape[1] // HD
    heads_local = queries.shape[1] // HD
    groups = heads_local // kv_local
    blocks = local_rows // WINDOW
    key_value = jnp.concatenate([keys, values], axis=1)
    previous = shifted(key_value[local_rows - WINDOW :], "sp", 1)
    extended = jnp.concatenate([previous, key_value], axis=0)
    stacked = extended.reshape(blocks + 1, WINDOW, 2 * kv_local * HD)
    band = jnp.concatenate([stacked[:-1], stacked[1:]], axis=1)
    key_band = band[:, :, : kv_local * HD].reshape(blocks, 2 * WINDOW, kv_local, HD)
    value_band = band[:, :, kv_local * HD :].reshape(blocks, 2 * WINDOW, kv_local, HD)
    query_blocks = queries.reshape(blocks, WINDOW, kv_local, groups, HD)
    query_index = jnp.arange(WINDOW, dtype=jnp.int32)[:, None]
    key_index = jnp.arange(2 * WINDOW, dtype=jnp.int32)[None, :]
    distance = query_index - key_index + WINDOW
    offset = lax.axis_index("sp") * local_rows
    key_place = (
        offset
        + jnp.arange(blocks, dtype=jnp.int32)[:, None, None] * WINDOW
        + key_index[None]
        - WINDOW
    )
    valid = (distance >= 0) & (distance < WINDOW) & (key_place >= 0)
    head_number = (
        lax.axis_index("tp") * heads_local + jnp.arange(heads_local, dtype=jnp.int32) + 1
    ).astype(jnp.float32)
    slopes = (2.0 ** (-8.0 * head_number / QH)).reshape(kv_local, groups, 1, 1, 1)
    scores = jnp.einsum(
        "nqhgd,nkhd->hgnqk", query_blocks, key_band, preferred_element_type=jnp.float32
    ) * HD ** (-0.5)
    scores = scores - slopes * distance.astype(jnp.float32)
    scores = jnp.where(valid, scores, -jnp.inf)
    sinks = sink_logits.reshape(kv_local, groups, 1, 1, 1)
    top = jnp.maximum(jnp.max(scores, axis=-1, keepdims=True), sinks)
    expd = jnp.exp(scores - top)
    denom = jnp.sum(expd, axis=-1, keepdims=True) + jnp.exp(sinks - top)
    weights = (expd / denom).astype(jnp.bfloat16)
    output = jnp.einsum(
        "hgnqk,nkhd->nqhgd", weights, value_band, preferred_element_type=jnp.float32
    )
    return output.reshape(local_rows, heads_local * HD).astype(jnp.bfloat16)


def rms_scale(rows, norm_gain):
    rows_f = rows.astype(jnp.float32)
    scale = lax.rsqrt(jnp.mean(rows_f * rows_f, axis=-1, keepdims=True) + 1e-06)
    return (rows_f * scale * norm_gain).astype(jnp.bfloat16)


def expand_rows(normed, gate_full, up_full):
    gate = jnp.dot(normed, gate_full, preferred_element_type=jnp.float32)
    upper = jnp.dot(normed, up_full, preferred_element_type=jnp.float32)
    return (jax.nn.silu(gate) * upper).astype(jnp.bfloat16)


def per_device(
    queries,
    keys,
    values,
    sink_logits,
    residual,
    out_weight,
    norm_gain,
    gate_weight,
    up_weight,
    down_weight,
):
    attended = attend(queries, keys, values, sink_logits)
    local_rows = queries.shape[0]
    tp_count = lax.axis_size("tp")
    own_rows = local_rows // tp_count
    first_row = lax.axis_index("tp") * own_rows
    partial_sum = jnp.dot(attended, out_weight, preferred_element_type=jnp.float32)
    projected = lax.psum(partial_sum.astype(jnp.bfloat16), "tp").astype(jnp.float32)
    mixed_all = (residual.astype(jnp.float32) + projected).astype(jnp.bfloat16)
    mixed_rows = lax.dynamic_slice_in_dim(mixed_all, first_row, own_rows, 0)
    gate_full, up_full = (
        lax.all_gather(gate_weight, "sp", axis=0, tiled=True),
        lax.all_gather(up_weight, "sp", axis=0, tiled=True),
    )
    hidden = expand_rows(rms_scale(mixed_all, norm_gain), gate_full, up_full)
    down_full = lax.all_gather(down_weight, "sp", axis=0, tiled=True)
    expanded = lax.psum_scatter(
        lax.dot_general(
            hidden, down_full, (((1,), (1,)), ((), ())), preferred_element_type=jnp.float32
        ).astype(jnp.bfloat16),
        "tp",
        scatter_dimension=0,
        tiled=True,
    ).astype(jnp.float32)
    return (mixed_rows.astype(jnp.float32) + 0.5 * expanded).astype(jnp.bfloat16)


def solution(mesh):
    return jax.shard_map(
        per_device,
        mesh=mesh,
        in_specs=(
            P("sp", "tp"),
            P("sp", "tp"),
            P("sp", "tp"),
            P("tp"),
            P("sp", None),
            P("tp", None),
            P(),
            P("sp", "tp"),
            P("sp", "tp"),
            P("sp", "tp"),
        ),
        out_specs=P(("sp", "tp"), None),
        check_vma=False,
    )
```

profile of v0, /device:TPU:0, one launch (start us, length us, event | category | flops | bytes accessed | tf_op | source)
XLA Modules:
  0.0 386.4 jit_solution(11114447815396450490)
XLA Ops:
  7.4 1.1 constant_dynamic-update-slice_fusion.1
  8.5 1.0 constant_dynamic-update-slice_fusion
  9.5 4.9 %collective-permute-start = (bf16[128,256]{1,0:T(8,128)(2,1)S(1)}, bf16[128,256]{1,0:T(8,128)(2,1)S(1)}, u32[]{:S(2)}, u32[]{:S(2)}) collective-permute-start(bf16[128,256]{1,0:T(8,128)(2,1)S(1)} %slice.25), channel_id=1, source_target_pairs={{0,4},{4,8},{8,12},{12,16},{16,20},{20,24},{24,28},{1,5},{5,9},{9,... | collective-permute-start | bytes 196616 | tf_op jit(solution)/shard_map/ppermute | solution.py:14
  14.7 0.3 broadcast_and_fusion
  15.0 3.2 reshape.128
  18.3 0.7 max.18
  19.5 2.3 fusion.5
  22.0 1.9 copy-done.1
  23.8 1.1 fusion.4
  25.3 3.5 fusion.11
  28.7 0.3 copy.26
  29.1 3.3 convolution_convert_fusion.1
  32.5 0.5 all-gather.4.cloned.1.call-update
  33.0 0.5 all-gather.6.cloned.1.call-update
  33.6 0.5 all-gather.8.cloned.1.call-update
  34.4 83.9 %all-reduce.2.cloned.1.call-done = bf16[1024,2048]{1,0:T(8,128)(2,1)} async-done(((bf16[1024,2048]{1,0:T(8,128)(2,1)}), bf16[1024,2048]{1,0:T(8,128)(2,1)}) %all-reduce.2.cloned.1.call-update) | async-done | bytes 4194320 | tf_op jit(solution)/shard_map/psum | solution.py:92
  118.4 7.5 %fusion = (f32[1024]{0:T(1024)S(1)}, bf16[1024,2048]{1,0:T(8,128)(2,1)}) fusion(bf16[1024,2048]{1,0:T(8,128)(2,1)} %all-reduce.2.cloned.1.call-done, bf16[1024,2048]{1,0:T(8,128)(2,1)} %param.14), kind=kLoop, calls=%fused_computation.2 | loop fusion | flops 14679040 | bytes 12587008 | tf_op jit(solution)/shard_map/reduce_sum | solution.py:64
  125.8 1.7 all-gather.4.cloned.1.call-done
  127.5 11.9 %fusion.15 = f32[1024,1408]{1,0:T(8,128)} fusion(bf16[2048,1408]{1,0:T(8,128)(2,1)} %all-gather.4.cloned.1.call-done, bf16[1024,2048]{1,0:T(8,128)(2,1)} %get-tuple-element.6, f32[2048]{0:T(1024)S(1)} %copy-done.2, f32[1024]{0:T(1024)S(1)} %add_rsqrt_fusion), kind=kOutput, calls=%fused_computation.20 | convolution fusion | flops 5913968640 | bytes 15740928 | tf_op jit(solution)/shard_map/dot_general | solution.py:69
  139.5 80.4 %all-gather.6.cloned.1.call-done = bf16[2048,1408]{1,0:T(8,128)(2,1)} async-done(((bf16[256,1408]{1,0:T(8,128)(2,1)}), bf16[2048,1408]{1,0:T(8,128)(2,1)}) %all-gather.6.cloned.1.call-update) | async-done | bytes 5767184 | tf_op jit(solution)/shard_map/all_gather | solution.py:97
  219.9 92.4 %all-gather.8.cloned.1.call-done = bf16[2048,1408]{1,0:T(8,128)(2,1)} async-done(((bf16[256,1408]{1,0:T(8,128)(2,1)}), bf16[2048,1408]{1,0:T(8,128)(2,1)}) %all-gather.8.cloned.1.call-update) | async-done | bytes 5767184 | tf_op jit(solution)/shard_map/all_gather | solution.py:100
  312.2 20.8 %convolution_convert_fusion = bf16[1024,2048]{1,0:T(8,128)(2,1)} fusion(bf16[2048,1408]{1,0:T(8,128)(2,1)} %all-gather.8.cloned.1.call-done, f32[1024,1408]{1,0:T(8,128)} %fusion.15, bf16[2048,1408]{1,0:T(8,128)(2,1)} %all-gather.6.cloned.1.call-done, bf16[1024,2048]{1,0:T(8,128)(2,1)} %get-tuple-element.6, f32[2048]{0:T(1024)S(1)} %copy-done.2, ...), kind=kOutput, calls=%fused_computation.11 | convolution fusion | flops 11830296576 | bytes 25702400 | tf_op jit(solution)/shard_map/dot_general | solution.py:102
  333.1 42.8 %reduce-scatter.2.cloned.1.call-done = bf16[256,2048]{1,0:T(8,128)(2,1)} async-done(((bf16[1024,2048]{1,0:T(8,128)(2,1)}), bf16[256,2048]{1,0:T(8,128)(2,1)}) %reduce-scatter.2.cloned.1.call-update) | async-done | bytes 1048592 | tf_op jit(solution)/shard_map/reduce_scatter | solution.py:101
  375.9 2.9 add_convert_fusion.1
  (27 shorter events, 1.6 us)
Async XLA Ops:
  7.4 21.7 %copy-start = (bf16[256,2048]{1,0:T(8,128)(2,1)S(1)}, bf16[256,2048]{1,0:T(8,128)(2,1)}, u32[]{:S(2)}) copy-start(bf16[256,2048]{1,0:T(8,128)(2,1)} %param.15) | copy-start | bytes 3145732
  7.4 111.0 %all-reduce.2.cloned.1.call-start = ((), (), s32[]{:S(2)}) async-start(), calls=%async_computation.1 | async-start | bytes 8388608 | tf_op jit(solution)/shard_map/psum | solution.py:92
  9.5 9.5 %collective-permute-start = (bf16[128,256]{1,0:T(8,128)(2,1)S(1)}, bf16[128,256]{1,0:T(8,128)(2,1)S(1)}, u32[]{:S(2)}, u32[]{:S(2)}) collective-permute-start(bf16[128,256]{1,0:T(8,128)(2,1)S(1)} %slice.25), channel_id=1, source_target_pairs={{0,4},{4,8},{8,12},{12,16},{16,20},{20,24},{24,28},{1,5},{5,9},{9,... | collective-permute-start | bytes 196616 | tf_op jit(solution)/shard_map/ppermute | solution.py:14
  21.9 1.9 copy-start.1
  32.4 95.1 %all-gather.4.cloned.1.call-start = ((), (), s32[]{:S(2)}) async-start(), calls=%async_computation.2 | async-start | bytes 6488064 | tf_op jit(solution)/shard_map/all_gather | solution.py:96
  33.0 186.9 %all-gather.6.cloned.1.call-start = ((), (), s32[]{:S(2)}) async-start(), calls=%async_computation.3 | async-start | bytes 6488064 | tf_op jit(solution)/shard_map/all_gather | solution.py:97
  33.6 278.7 %all-gather.8.cloned.1.call-start = ((), (), s32[]{:S(2)}) async-start(), calls=%async_computation.4 | async-start | bytes 6488064 | tf_op jit(solution)/shard_map/all_gather | solution.py:100
  34.2 93.4 %copy-start.2 = (f32[2048]{0:T(1024)S(1)}, f32[2048]{0:T(1024)}, u32[]{:S(2)}) copy-start(f32[2048]{0:T(1024)} %param.16) | copy-start | bytes 24580
  34.2 341.8 %reduce-scatter.2.cloned.1.call-start = ((), (), s32[]{:S(2)}) async-start(), calls=%async_computation.5 | async-start | bytes 5242880 | tf_op jit(solution)/shard_map/reduce_scatter | solution.py:101
Sparse Core Ops, SparseCore 0:
  32.5 85.7 all-reduce.1
  333.2 42.6 reduce-scatter.1
Sparse Core Ops, SparseCore 1:
  35.1 92.4 all-gather.3
  129.6 90.2 all-gather.5
  222.0 90.2 all-gather.7
where the time goes:
time: 387 us; the launch traced here: 386 us
  waiting for transfers between devices  303 us (78%)
  matrix products  41.9 us (11%)
  between operations  15.2 us (4%)
  other arithmetic  12.5 us (3%)
  local copies, waits for them, and re-layouts  8.71 us (2%)
  starting transfers between devices  5.25 us (1%)
    all_gather x1, waiting for transfers between devices, per_device(): down_full = lax.all_gather(down_weight, 'sp', axis=0, tiled=True)  92.4 us
    psum x1, waiting for transfers between devices, per_device(): lax.psum(partial_sum.astype(jnp.bfloat16), 'tp').astype(jnp.float32)  83.9 us
    all_gather x1, waiting for transfers between devices, per_device(): lax.all_gather(up_weight, 'sp', axis=0, tiled=True)  80.4 us
    reduce_scatter x1, waiting for transfers between devices, per_device(): lax.psum_scatter(lax.dot_general(hidden, down_full, (((1,), (1,)), ((), (...  42.8 us
    dot_general x1, matrix products, per_device(): lax.dot_general(hidden, down_full, (((1,), (1,)), ((), ())), preferred_el...  20.8 us
    dot_general x1, matrix products, expand_rows(): gate = jnp.dot(normed, gate_full, preferred_element_type=jnp.float32)  11.9 us
  transfers between devices with their start and end apart: 6, of which 5 were waited for; matrix products, arithmetic and copies ran while one was open for 6% of the time, Pallas kernels for 0%

commit v1 on v0

--- a/solution.py
+++ b/solution.py
@@ -97,7 +97,12 @@
         lax.all_gather(up_weight, "sp", axis=0, tiled=True),
     )
     hidden = expand_rows(rms_scale(mixed_all, norm_gain), gate_full, up_full)
-    down_full = lax.all_gather(down_weight, "sp", axis=0, tiled=True)
+    ring = [down_weight]
+    for hop in range(7):
+        ring.append(lax.ppermute(ring[-1], "sp", [(dev, (dev + 1) % 8) for dev in range(8)]))
+    down_full = jnp.roll(
+        jnp.concatenate(ring[::-1], axis=0), (lax.axis_index("sp") + 1) * ring[0].shape[0], axis=0
+    )
     expanded = lax.psum_scatter(
         lax.dot_general(
             hidden, down_full, (((1,), (1,)), ((), ())), preferred_element_type=jnp.float32

time: 387 us -> 366 us (0.946)
  waiting for transfers between devices: 303 us -> 262 us
  local copies, waits for them, and re-layouts: 8.71 us -> 29.3 us
    ppermute x0 -> x7, waiting for transfers between devices: none -> 200 us  [per_device(): lax.ppermute(ring[-1], 'sp', [(dev, (dev + 1) % 8) for dev in range(8)])]
    all_gather x1 -> x0, waiting for transfers between devices: 92.4 us -> none  [per_device(): down_full = lax.all_gather(down_weight, 'sp', axis=0, tiled=True)]
    psum x1, waiting for transfers between devices: 83.9 us -> 0.01 us  [per_device(): lax.psum(partial_sum.astype(jnp.bfloat16), 'tp').astype(jnp.float32)]
    all_gather x1, waiting for transfers between devices: 80.4 us -> 18.3 us  [per_device(): lax.all_gather(up_weight, 'sp', axis=0, tiled=True)]
    unnamed x7 -> x28, local copies, waits for them, and re-layouts: 2.95 us -> 22.6 us
  transfers between devices with their start and end apart: 6 -> 12, of which waited for: 5 -> 9; matrix products, arithmetic and copies ran while one was open for 6% -> 12% of each run, Pallas kernels for 0% -> 0%
where the time goes in v1:
time: 366 us
  waiting for transfers between devices  262 us (72%)
  matrix products  39.8 us (11%)
  local copies, waits for them, and re-layouts  29.3 us (8%)
  between operations  15 us (4%)
  other arithmetic  12.6 us (3%)
  starting transfers between devices  7.53 us (2%)
    ppermute x7, waiting for transfers between devices, per_device(): lax.ppermute(ring[-1], 'sp', [(dev, (dev + 1) % 8) for dev in range(8)])  200 us
    reduce_scatter x1, waiting for transfers between devices, per_device(): lax.psum_scatter(lax.dot_general(hidden, down_full, (((1,), (1,)), ((), (...  43.2 us
    unnamed x28, local copies, waits for them, and re-layouts  22.6 us
    dot_general x1, matrix products, per_device(): lax.dot_general(hidden, down_full, (((1,), (1,)), ((), ())), preferred_el...  20.9 us
    all_gather x1, waiting for transfers between devices, per_device(): lax.all_gather(up_weight, 'sp', axis=0, tiled=True)  18.3 us
    dot_general x1, matrix products, expand_rows(): gate = jnp.dot(normed, gate_full, preferred_element_type=jnp.float32)  11.9 us
    reduce_sum x1, other arithmetic, rms_scale(): scale = lax.rsqrt(jnp.mean(rows_f * rows_f, axis=-1, keepdims=True) + 1e-06)  7.52 us
  transfers between devices with their start and end apart: 12, of which 9 were waited for; matrix products, arithmetic and copies ran while one was open for 12% of the time, Pallas kernels for 0%

profile of v1, /device:TPU:0, one launch (start us, length us, event | category | flops | bytes accessed | tf_op | source)
XLA Modules:
  0.0 365.8 jit_solution(1417598632741641542)
XLA Ops:
  9.5 4.9 %collective-permute-start = (bf16[128,256]{1,0:T(8,128)(2,1)S(1)}, bf16[128,256]{1,0:T(8,128)(2,1)S(1)}, u32[]{:S(2)}, u32[]{:S(2)}) collective-permute-start(bf16[128,256]{1,0:T(8,128)(2,1)S(1)} %slice.25), channel_id=1, source_target_pairs={{0,4},{4,8},{8,12},{12,16},{16,20},{20,24},{24,28},{1,5},{5,9},{9,... | collective-permute-start | bytes 196616 | tf_op jit(solution)/shard_map/ppermute | solution.py:14
  15.0 3.2 reshape.128
  19.8 2.3 fusion.10
  25.0 3.3 convolution_convert_fusion
  29.0 1.6 collective-permute-start.1
  30.6 24.3 %collective-permute-done.1 = bf16[256,1408]{1,0:T(8,128)(2,1)S(1)} collective-permute-done((bf16[256,1408]{1,0:T(8,128)(2,1)S(1)}, bf16[256,1408]{1,0:T(8,128)(2,1)S(1)}, u32[]{:S(2)}, u32[]{:S(2)}) %collective-permute-start.1) | collective-permute-done | bytes 720928 | tf_op jit(solution)/shard_map/ppermute | solution.py:102
  55.9 32.2 %collective-permute-done.2 = bf16[256,1408]{1,0:T(8,128)(2,1)S(1)} collective-permute-done((bf16[256,1408]{1,0:T(8,128)(2,1)S(1)}, bf16[256,1408]{1,0:T(8,128)(2,1)S(1)}, u32[]{:S(2)}, u32[]{:S(2)}) %collective-permute-start.2) | collective-permute-done | bytes 720928 | tf_op jit(solution)/shard_map/ppermute | solution.py:102
  88.1 35.0 %collective-permute-done.3 = bf16[256,1408]{1,0:T(8,128)(2,1)S(1)} collective-permute-done((bf16[256,1408]{1,0:T(8,128)(2,1)S(1)}, bf16[256,1408]{1,0:T(8,128)(2,1)S(1)}, u32[]{:S(2)}, u32[]{:S(2)}) %collective-permute-start.3) | collective-permute-done | bytes 720928 | tf_op jit(solution)/shard_map/ppermute | solution.py:102
  123.0 35.1 %collective-permute-done.4 = bf16[256,1408]{1,0:T(8,128)(2,1)S(1)} collective-permute-done((bf16[256,1408]{1,0:T(8,128)(2,1)S(1)}, bf16[256,1408]{1,0:T(8,128)(2,1)S(1)}, u32[]{:S(2)}, u32[]{:S(2)}) %collective-permute-start.4) | collective-permute-done | bytes 720928 | tf_op jit(solution)/shard_map/ppermute | solution.py:102
  159.0 24.7 %collective-permute-done.5 = bf16[256,1408]{1,0:T(8,128)(2,1)} collective-permute-done((bf16[256,1408]{1,0:T(8,128)(2,1)S(1)}, bf16[256,1408]{1,0:T(8,128)(2,1)}, u32[]{:S(2)}, u32[]{:S(2)}) %collective-permute-start.5) | collective-permute-done | bytes 720928 | tf_op jit(solution)/shard_map/ppermute | solution.py:102
  183.7 32.8 %collective-permute-done.6 = bf16[256,1408]{1,0:T(8,128)(2,1)} collective-permute-done((bf16[256,1408]{1,0:T(8,128)(2,1)}, bf16[256,1408]{1,0:T(8,128)(2,1)}, u32[]{:S(2)}, u32[]{:S(2)}) %collective-permute-start.6) | collective-permute-done | bytes 720928 | tf_op jit(solution)/shard_map/ppermute | solution.py:102
  216.5 7.5 %fusion = (f32[1024]{0:T(1024)S(1)}, bf16[1024,2048]{1,0:T(8,128)(2,1)}) fusion(bf16[1024,2048]{1,0:T(8,128)(2,1)} %all-reduce.2.cloned.1.call-done, bf16[1024,2048]{1,0:T(8,128)(2,1)} %param.14), kind=kLoop, calls=%fused_computation.2 | loop fusion | flops 14679040 | bytes 12587008 | tf_op jit(solution)/shard_map/reduce_sum | solution.py:64
  224.0 15.5 %collective-permute-done.7 = bf16[256,1408]{1,0:T(8,128)(2,1)} collective-permute-done((bf16[256,1408]{1,0:T(8,128)(2,1)}, bf16[256,1408]{1,0:T(8,128)(2,1)}, u32[]{:S(2)}, u32[]{:S(2)}) %collective-permute-start.7) | collective-permute-done | bytes 720928 | tf_op jit(solution)/shard_map/ppermute | solution.py:102
  239.5 2.1 constant_dynamic-update-slice_fusion.17
  241.6 2.0 constant_dynamic-update-slice_fusion.16
  243.6 2.1 constant_dynamic-update-slice_fusion.15
  250.3 2.1 constant_dynamic-update-slice_fusion.9
  252.4 2.0 constant_dynamic-update-slice_fusion.8
  254.4 2.0 constant_dynamic-update-slice_fusion.7
  261.1 11.9 %fusion.20 = f32[1024,1408]{1,0:T(8,128)} fusion(bf16[2048,1408]{1,0:T(8,128)(2,1)} %all-gather.3.cloned.1.call-done, bf16[1024,2048]{1,0:T(8,128)(2,1)} %get-tuple-element.6, f32[2048]{0:T(1024)S(1)} %copy-done.5, f32[1024]{0:T(1024)S(1)} %add_rsqrt_fusion), kind=kOutput, calls=%fused_computation.22 | convolution fusion | flops 5913968640 | bytes 15740928 | tf_op jit(solution)/shard_map/dot_general | solution.py:69
  273.0 18.3 %all-gather.5.cloned.1.call-done = bf16[2048,1408]{1,0:T(8,128)(2,1)} async-done(((bf16[256,1408]{1,0:T(8,128)(2,1)}), bf16[2048,1408]{1,0:T(8,128)(2,1)}) %all-gather.5.cloned.1.call-update) | async-done | bytes 5767184 | tf_op jit(solution)/shard_map/all_gather | solution.py:97
  291.3 20.9 %fusion.6 = bf16[1024,2048]{1,0:T(8,128)(2,1)} fusion(bf16[4096,1408]{1,0:T(8,128)(2,1)} %constant_dynamic-update-slice_fusion.2, s32[]{:T(128)S(6)} %select_n.23, f32[1024,1408]{1,0:T(8,128)} %fusion.20, bf16[2048,1408]{1,0:T(8,128)(2,1)} %all-gather.5.cloned.1.call-done, bf16[1024,2048]{1,0:T(8,128)(2,1)} %get-tuple-element.6, f32[2048]{0:T(1024)S(1)} %copy-done.5, ...), kind=kOutput, calls=%fused_computation.13 | convolution fusion | flops 11830296576 | bytes 25702404 | tf_op jit(solution)/shard_map/dot_general | solution.py:107
  312.3 43.2 %reduce-scatter.2.cloned.1.call-done = bf16[256,2048]{1,0:T(8,128)(2,1)} async-done(((bf16[1024,2048]{1,0:T(8,128)(2,1)}), bf16[256,2048]{1,0:T(8,128)(2,1)}) %reduce-scatter.2.cloned.1.call-update) | async-done | bytes 1048592 | tf_op jit(solution)/shard_map/reduce_scatter | solution.py:106
  355.4 2.9 add_convert_fusion.1
  (60 shorter events, 18.9 us)
Async XLA Ops:
  7.4 17.6 %copy-start = (bf16[256,2048]{1,0:T(8,128)(2,1)S(1)}, bf16[256,2048]{1,0:T(8,128)(2,1)}, u32[]{:S(2)}) copy-start(bf16[256,2048]{1,0:T(8,128)(2,1)} %param.15) | copy-start | bytes 3145732
  7.4 209.1 %all-reduce.2.cloned.1.call-start = ((), (), s32[]{:S(2)}) async-start(), calls=%async_computation.1 | async-start | bytes 8388608 | tf_op jit(solution)/shard_map/psum | solution.py:92
  9.5 9.5 %collective-permute-start = (bf16[128,256]{1,0:T(8,128)(2,1)S(1)}, bf16[128,256]{1,0:T(8,128)(2,1)S(1)}, u32[]{:S(2)}, u32[]{:S(2)}) collective-permute-start(bf16[128,256]{1,0:T(8,128)(2,1)S(1)} %slice.25), channel_id=1, source_target_pairs={{0,4},{4,8},{8,12},{12,16},{16,20},{20,24},{24,28},{1,5},{5,9},{9,... | collective-permute-start | bytes 196616 | tf_op jit(solution)/shard_map/ppermute | solution.py:14
  25.0 4.0 %copy-start.2 = (bf16[256,1408]{1,0:T(8,128)(2,1)S(1)}, bf16[256,1408]{1,0:T(8,128)(2,1)}, u32[]{:S(2)}) copy-start(bf16[256,1408]{1,0:T(8,128)(2,1)} %param.19) | copy-start | bytes 2162692
  28.4 232.7 %all-gather.3.cloned.1.call-start = ((), (), s32[]{:S(2)}) async-start(), calls=%async_computation.2 | async-start | bytes 6488064 | tf_op jit(solution)/shard_map/all_gather | solution.py:96
  28.9 262.3 %all-gather.5.cloned.1.call-start = ((), (), s32[]{:S(2)}) async-start(), calls=%async_computation.3 | async-start | bytes 6488064 | tf_op jit(solution)/shard_map/all_gather | solution.py:97
  29.0 25.9 %collective-permute-start.1 = (bf16[256,1408]{1,0:T(8,128)(2,1)S(1)}, bf16[256,1408]{1,0:T(8,128)(2,1)S(1)}, u32[]{:S(2)}, u32[]{:S(2)}) collective-permute-start(bf16[256,1408]{1,0:T(8,128)(2,1)S(1)} %copy-done.2), channel_id=1, source_target_pairs={{0,4},{4,8},{8,12},{12,16},{16,20},{20,24},{24,28},{28,0},{1,5},{5... | collective-permute-start | bytes 2162696 | tf_op jit(solution)/shard_map/ppermute | solution.py:102
  54.9 33.2 %collective-permute-start.2 = (bf16[256,1408]{1,0:T(8,128)(2,1)S(1)}, bf16[256,1408]{1,0:T(8,128)(2,1)S(1)}, u32[]{:S(2)}, u32[]{:S(2)}) collective-permute-start(bf16[256,1408]{1,0:T(8,128)(2,1)S(1)} %collective-permute-done.1), channel_id=1, source_target_pairs={{0,4},{4,8},{8,12},{12,16},{16,20},{20,24},{24,28},{28,0},{1,5},{5... | collective-permute-start | bytes 2162696 | tf_op jit(solution)/shard_map/ppermute | solution.py:102
  55.8 299.6 %reduce-scatter.2.cloned.1.call-start = ((), (), s32[]{:S(2)}) async-start(), calls=%async_computation.4 | async-start | bytes 5242880 | tf_op jit(solution)/shard_map/reduce_scatter | solution.py:106
  88.1 35.0 %collective-permute-start.3 = (bf16[256,1408]{1,0:T(8,128)(2,1)S(1)}, bf16[256,1408]{1,0:T(8,128)(2,1)S(1)}, u32[]{:S(2)}, u32[]{:S(2)}) collective-permute-start(bf16[256,1408]{1,0:T(8,128)(2,1)S(1)} %collective-permute-done.2), channel_id=1, source_target_pairs={{0,4},{4,8},{8,12},{12,16},{16,20},{20,24},{24,28},{28,0},{1,5},{5... | collective-permute-start | bytes 2162696 | tf_op jit(solution)/shard_map/ppermute | solution.py:102
  123.0 35.1 %collective-permute-start.4 = (bf16[256,1408]{1,0:T(8,128)(2,1)S(1)}, bf16[256,1408]{1,0:T(8,128)(2,1)S(1)}, u32[]{:S(2)}, u32[]{:S(2)}) collective-permute-start(bf16[256,1408]{1,0:T(8,128)(2,1)S(1)} %collective-permute-done.3), channel_id=1, source_target_pairs={{0,4},{4,8},{8,12},{12,16},{16,20},{20,24},{24,28},{28,0},{1,5},{5... | collective-permute-start | bytes 2162696 | tf_op jit(solution)/shard_map/ppermute | solution.py:102
  158.1 0.9 copy-start.3
  159.0 24.7 %collective-permute-start.5 = (bf16[256,1408]{1,0:T(8,128)(2,1)S(1)}, bf16[256,1408]{1,0:T(8,128)(2,1)}, u32[]{:S(2)}, u32[]{:S(2)}) collective-permute-start(bf16[256,1408]{1,0:T(8,128)(2,1)S(1)} %collective-permute-done.4), channel_id=1, source_target_pairs={{0,4},{4,8},{8,12},{12,16},{16,20},{20,24},{24,28},{28,0},{1,5},{5... | collective-permute-start | bytes 2162696 | tf_op jit(solution)/shard_map/ppermute | solution.py:102
  183.7 32.8 %collective-permute-start.6 = (bf16[256,1408]{1,0:T(8,128)(2,1)}, bf16[256,1408]{1,0:T(8,128)(2,1)}, u32[]{:S(2)}, u32[]{:S(2)}) collective-permute-start(bf16[256,1408]{1,0:T(8,128)(2,1)} %collective-permute-done.5), channel_id=1, source_target_pairs={{0,4},{4,8},{8,12},{12,16},{16,20},{20,24},{24,28},{28,0},{1,5},{5... | collective-permute-start | bytes 2162696 | tf_op jit(solution)/shard_map/ppermute | solution.py:102
  216.5 23.0 %collective-permute-start.7 = (bf16[256,1408]{1,0:T(8,128)(2,1)}, bf16[256,1408]{1,0:T(8,128)(2,1)}, u32[]{:S(2)}, u32[]{:S(2)}) collective-permute-start(bf16[256,1408]{1,0:T(8,128)(2,1)} %collective-permute-done.6), channel_id=1, source_target_pairs={{0,4},{4,8},{8,12},{12,16},{16,20},{20,24},{24,28},{28,0},{1,5},{5... | collective-permute-start | bytes 2162696 | tf_op jit(solution)/shard_map/ppermute | solution.py:102
  216.5 29.1 %copy-start.4 = (bf16[256,1408]{1,0:T(8,128)(2,1)S(1)}, bf16[256,1408]{1,0:T(8,128)(2,1)}, u32[]{:S(2)}) copy-start(bf16[256,1408]{1,0:T(8,128)(2,1)} %copy-done.3) | copy-start | bytes 2162692
  250.3 10.8 %copy-start.5 = (f32[2048]{0:T(1024)S(1)}, f32[2048]{0:T(1024)}, u32[]{:S(2)}) copy-start(f32[2048]{0:T(1024)} %param.16) | copy-start | bytes 24580
  291.3 67.0 %copy-start.1 = (bf16[256,2048]{1,0:T(8,128)(2,1)S(1)}, bf16[256,2048]{1,0:T(8,128)(2,1)}, u32[]{:S(2)}) copy-start(bf16[256,2048]{1,0:T(8,128)(2,1)} %param.15) | copy-start | bytes 3145732
Sparse Core Ops, SparseCore 0:
  28.5 85.7 all-reduce.1
  312.4 42.9 reduce-scatter.1
Sparse Core Ops, SparseCore 1:
  31.0 136.0 all-gather.2
  169.2 122.1 all-gather.4
